TPU v7x, 32 devices: a whole 2x2x4 slice. The times are simulated.
32 devices in a mesh: grp: 2 (over y), fs: 4 (over z), tp: 4 (over x, core).
Axes of the slice: x: 2, y: 2, z: 4, core: 2. Of those that a mesh axis runs over, the one named last changes fastest.
Arguments:
- prompt: bfloat16 [1024, 2048], P(('grp', 'fs', 'tp')), parts along dimension 0, may hold values from -6 to 6
- norm_gain: float32 [2048], P('fs'), may hold values from 0.1 to 1.9
- up_weight: float32 [2048, 8192], P('fs', 'tp'), may hold values from -0.125 to 0.125
- down_weight: float32 [8192, 2048], P('fs', 'tp'), may hold values from -0.0625 to 0.0625
Outputs:
- up_serving: bfloat16 [4096, 8192], P('grp', 'fs'), parts along dimension 0
- down_serving: bfloat16 [8192, 4096], P('fs', 'grp'), parts along dimension 1
- mlp_output: bfloat16 [1024, 2048], P(('grp', 'fs', 'tp')), parts along dimension 0
There are 2 independent parts, one for each index of `grp`. A program takes and returns all parts, laid end to end along the dimension named above; an argument that names none is the same for every part. Nothing has to cross between parts.
All inputs are finite; a program needn't handle non-finite values.
Results may differ from a plain program's by a relative error of at most 0.024.
Values may be sent and summed in bfloat16 or wider, within the bound.
A program may use at most 128 MiB of HBM per device.

v0:
```python
import jax
import jax.numpy as jnp
from jax import lax
from jax.sharding import PartitionSpec as P

epsilon = 1e-06


def per_device(prompt, norm_gain, up_weight, down_weight):
    folded = (norm_gain[:, None] * up_weight).astype(jnp.bfloat16)
    down_local = down_weight.astype(jnp.bfloat16)
    down_serving = lax.all_gather(down_local, "tp", axis=1, tiled=True)
    thin_rows = lax.all_to_all(folded, "tp", split_axis=0, concat_axis=1, tiled=True)
    crossed = lax.all_to_all(thin_rows, "fs", split_axis=1, concat_axis=0, tiled=True)
    stacked = lax.all_gather(crossed, "tp", axis=0, tiled=True)
    tp_count = lax.axis_size("tp")
    fs_count = lax.axis_size("fs")
    slice_height = folded.shape[0] // tp_count
    unit_count = stacked.shape[1]
    up_serving = stacked.reshape(tp_count, fs_count, slice_height, unit_count)
    up_serving = up_serving.transpose(1, 0, 2, 3).reshape(-1, unit_count)
    widened = prompt.astype(jnp.float32)
    normed = (
        widened * lax.rsqrt(jnp.mean(widened * widened, axis=-1, keepdims=True) + epsilon)
    ).astype(jnp.bfloat16)
    projected = jnp.dot(
        lax.all_gather(normed, "fs", axis=0, tiled=True),
        up_serving,
        preferred_element_type=jnp.float32,
    )
    hidden = jnp.square(jax.nn.relu(projected)).astype(jnp.bfloat16)
    summed = lax.psum_scatter(
        jnp.dot(hidden, down_serving, preferred_element_type=jnp.float32).astype(jnp.bfloat16),
        "fs",
        scatter_dimension=0,
        tiled=True,
    )
    return (up_serving, down_serving, summed)


def solution(mesh):
    return jax.shard_map(
        per_device,
        mesh=mesh,
        in_specs=(P(("grp", "fs", "tp"), None), P("fs"), P("fs", "tp"), P("fs", "tp")),
        out_specs=(P("grp", "fs"), P("fs", "grp"), P(("grp", "fs", "tp"), None)),
        check_vma=False,
    )
```

profile of v0, /device:TPU:0, one launch (start us, length us, event | category | flops | bytes accessed | tf_op | source)
XLA Modules:
  0.0 255.5 jit_solution(17152566268026169703)
XLA Ops:
  7.2 0.0 all-gather.3.cloned.1.call-start
  7.2 2.5 multiply_convert_fusion
  9.7 29.7 %all_to_all.32 = bf16[4,128,2048]{2,1,0:T(8,128)(2,1)S(1)} all-to-all(bf16[4,128,2048]{2,1,0:T(8,128)(2,1)S(1)} %bitcast.17), channel_id=1, replica_groups=mesh['grp'=2,'fs'=4,'tp'=4] {'tp'}, dimensions={0} | all-to-all | bytes 4194304 | tf_op jit(solution)/shard_map/all_to_all | solution.py:13
  39.4 0.0 copy-start
  39.4 52.7 %all_to_all.33 = bf16[128,4,2048]{2,0,1:T(8,128)(2,1)} all-to-all(bf16[128,4,2048]{2,0,1:T(8,128)(2,1)S(1)} %bitcast.16), channel_id=1, replica_groups=mesh['grp'=2,'fs'=4,'tp'=4] {'fs'}, dimensions={1} | all-to-all | bytes 4194304 | tf_op jit(solution)/shard_map/all_to_all | solution.py:14
  92.1 0.0 all-gather.3.cloned.1.call-update
  92.1 0.0 all-gather.5.cloned.1.call-start
  92.2 3.8 %convert_element_type.19 = bf16[2048,512]{1,0:T(8,128)(2,1)} convert(f32[2048,512]{1,0:T(8,128)} %param.7) | non-fusion elementwise | flops 1048576 | bytes 6291456 | tf_op jit(solution)/shard_map/convert_element_type | solution.py:11
  96.0 0.0 all-gather.5.cloned.1.call-update
  96.0 0.0 reduce-scatter.2.cloned.1.call-start
  96.0 0.0 copy-done
  96.1 0.1 fusion.3
  96.2 0.1 fusion.4
  96.3 15.7 %all_gather.11 = bf16[128,2048]{1,0:T(8,128)(2,1)S(1)} all-gather(bf16[32,2048]{1,0:T(8,128)(2,1)S(1)} %fusion.4), channel_id=1, replica_groups=mesh['grp'=2,'fs'=4,'tp'=4] {'fs'}, dimensions={0}, use_global_device_ids=true | all-gather | bytes 655360 | tf_op jit(solution)/shard_map/all_gather | solution.py:27
  112.0 37.2 %all-gather.3.cloned.1.call-done = bf16[2048,2048]{1,0:T(8,128)(2,1)} async-done(((bf16[512,2048]{1,0:T(8,128)(2,1)}), bf16[2048,2048]{1,0:T(8,128)(2,1)}) %all-gather.3.cloned.1.call-update) | async-done | bytes 8388624 | tf_op jit(solution)/shard_map/all_gather | solution.py:15
  149.2 8.4 %copy.7 = bf16[4,4,128,2048]{3,2,1,0:T(8,128)(2,1)} copy(bf16[4,4,128,2048]{3,2,0,1:T(8,128)(2,1)} %bitcast.14) | data formatting | bytes 16777216 | tf_op jit(solution)/shard_map/transpose | solution.py:21
  157.6 52.0 %all-gather.5.cloned.1.call-done = bf16[2048,2048]{1,0:T(8,128)(2,1)} async-done(((bf16[2048,512]{1,0:T(8,128)(2,1)}), bf16[2048,2048]{1,0:T(8,128)(2,1)}) %all-gather.5.cloned.1.call-update) | async-done | bytes 8388624 | tf_op jit(solution)/shard_map/all_gather | solution.py:12
  209.6 8.9 %convolution_convert_fusion = bf16[128,2048]{1,0:T(8,128)(2,1)} fusion(bf16[2048,2048]{1,0:T(8,128)(2,1)} %all-gather.5.cloned.1.call-done, bf16[128,2048]{1,0:T(8,128)(2,1)S(1)} %all_gather.11, bf16[2048,2048]{1,0:T(8,128)(2,1)} %bitcast.12), kind=kOutput, calls=%fused_computation.3 | convolution fusion | flops 2148532224 | bytes 17825792 | tf_op jit(solution)/shard_map/dot_general | solution.py:33
  218.5 0.0 reduce-scatter.2.cloned.1.call-update
  218.5 22.0 %reduce-scatter.2.cloned.1.call-done = bf16[32,2048]{1,0:T(8,128)(2,1)} async-done(((bf16[128,2048]{1,0:T(8,128)(2,1)}), bf16[32,2048]{1,0:T(8,128)(2,1)}) %reduce-scatter.2.cloned.1.call-update) | async-done | bytes 131088 | tf_op jit(solution)/shard_map/reduce_scatter | solution.py:32
  240.5 8.4 %copy.9 = bf16[2048,2048]{1,0:T(8,128)(2,1)} copy(bf16[2048,2048]{1,0:T(8,128)(2,1)} %all-gather.5.cloned.1.call-done) | data formatting | bytes 16777216
  (1 shorter events, 0.0 us)
Async XLA Ops:
  7.2 142.0 %all-gather.3.cloned.1.call-start = ((), (), s32[]{:S(2)}) async-start(), calls=%async_computation.3 | async-start | bytes 10485760 | tf_op jit(solution)/shard_map/all_gather | solution.py:15
  39.4 56.7 %copy-start = (bf16[32,2048]{1,0:T(8,128)(2,1)S(1)}, bf16[32,2048]{1,0:T(8,128)(2,1)}, u32[]{:S(2)}) copy-start(bf16[32,2048]{1,0:T(8,128)(2,1)} %param.4) | copy-start | bytes 393220
  92.1 117.4 %all-gather.5.cloned.1.call-start = ((), (), s32[]{:S(2)}) async-start(), calls=%async_computation.4 | async-start | bytes 10485760 | tf_op jit(solution)/shard_map/all_gather | solution.py:12
  96.0 144.5 %reduce-scatter.2.cloned.1.call-start = ((), (), s32[]{:S(2)}) async-start(), calls=%async_computation.5 | async-start | bytes 655360 | tf_op jit(solution)/shard_map/reduce_scatter | solution.py:32
Sparse Core Ops, SparseCore 0:
  92.3 56.8 all-gather.2
  151.3 58.2 all-gather.4
  218.7 21.8 reduce-scatter.1
where the time goes:
time: 256 us; the launch traced here: 255 us
  waiting for transfers between devices  111 us (43%)
  blocking collectives  98.1 us (38%)
  local copies, waits for them, and re-layouts  16.9 us (7%)
  between operations  13.8 us (5%)
  matrix products  8.93 us (3%)
  other arithmetic  6.49 us (3%)
    all_to_all x1, blocking collectives, per_device(): lax.all_to_all(thin_rows, 'fs', split_axis=1, concat_axis=0, tiled=True)  52.7 us
    all_gather x1, waiting for transfers between devices, per_device(): down_serving = lax.all_gather(down_local, 'tp', axis=1, tiled=True)  52 us
    all_gather x1, waiting for transfers between devices, per_device(): stacked = lax.all_gather(crossed, 'tp', axis=0, tiled=True)  37.2 us
    all_to_all x1, blocking collectives, per_device(): lax.all_to_all(folded, 'tp', split_axis=0, concat_axis=1, tiled=True)  29.7 us
    reduce_scatter x1, waiting for transfers between devices, per_device(): lax.psum_scatter(jnp.dot(hidden, down_serving, preferred_element_type=jnp...  22 us
    all_gather x1, blocking collectives, per_device(): lax.all_gather(normed, 'fs', axis=0, tiled=True)  15.7 us
    dot_general x1, matrix products, per_device(): jnp.dot(hidden, down_serving, preferred_element_type=jnp.float32)  8.93 us
    unnamed x3, local copies, waits for them, and re-layouts  8.44 us
  transfers between devices with their start and end apart: 3, of which 3 were waited for; matrix products, arithmetic and copies ran while one was open for 5% of the time, Pallas kernels for 0%

commit v1 on v0

--- a/solution.py
+++ b/solution.py
@@ -9,7 +9,8 @@
 def per_device(prompt, norm_gain, up_weight, down_weight):
     folded = (norm_gain[:, None] * up_weight).astype(jnp.bfloat16)
     down_local = down_weight.astype(jnp.bfloat16)
-    down_serving = lax.all_gather(down_local, "tp", axis=1, tiled=True)
+    pieces = lax.all_gather(down_local, "tp", axis=0, tiled=False)
+    down_serving = jnp.concatenate(pieces, axis=1)
     thin_rows = lax.all_to_all(folded, "tp", split_axis=0, concat_axis=1, tiled=True)
     crossed = lax.all_to_all(thin_rows, "fs", split_axis=1, concat_axis=0, tiled=True)
     stacked = lax.all_gather(crossed, "tp", axis=0, tiled=True)

time: 256 us -> 217 us (0.85)
  waiting for transfers between devices: 111 us -> 40.2 us
  blocking collectives: 98.1 us -> 116 us
  local copies, waits for them, and re-layouts: 16.9 us -> 31 us
    all_gather x1, waiting for transfers between devices: 52 us -> 0.01 us  [per_device(): pieces = lax.all_gather(down_local, 'tp', axis=0, tiled=False)]
    all_gather x1, waiting for transfers between devices: 37.2 us -> 18.1 us  [per_device(): stacked = lax.all_gather(crossed, 'tp', axis=0, tiled=True)]
    all_to_all x1, blocking collectives: 29.7 us -> 48.1 us  [per_device(): lax.all_to_all(folded, 'tp', split_axis=0, concat_axis=1, tiled=True)]
    all_gather x0 -> x1, local copies, waits for them, and re-layouts: none -> 12.2 us  [per_device(): pieces = lax.all_gather(down_local, 'tp', axis=0, tiled=False)]
    unnamed x3 -> x5, local copies, waits for them, and re-layouts: 8.44 us -> 10.4 us
  transfers between devices with their start and end apart: 3 -> 3, of which waited for: 3 -> 2; matrix products, arithmetic and copies ran while one was open for 5% -> 12% of each run, Pallas kernels for 0% -> 0%
where the time goes in v1:
time: 217 us
  blocking collectives  116 us (53%)
  waiting for transfers between devices  40.2 us (19%)
  local copies, waits for them, and re-layouts  31 us (14%)
  between operations  13.8 us (6%)
  matrix products  8.92 us (4%)
  other arithmetic  6.49 us (3%)
    all_to_all x1, blocking collectives, per_device(): lax.all_to_all(thin_rows, 'fs', split_axis=1, concat_axis=0, tiled=True)  52.6 us
    all_to_all x1, blocking collectives, per_device(): lax.all_to_all(folded, 'tp', split_axis=0, concat_axis=1, tiled=True)  48.1 us
    reduce_scatter x1, waiting for transfers between devices, per_device(): lax.psum_scatter(jnp.dot(hidden, down_serving, preferred_element_type=jnp...  22 us
    all_gather x1, waiting for transfers between devices, per_device(): stacked = lax.all_gather(crossed, 'tp', axis=0, tiled=True)  18.1 us
    all_gather x1, blocking collectives, per_device(): lax.all_gather(normed, 'fs', axis=0, tiled=True)  15.7 us
    all_gather x1, local copies, waits for them, and re-layouts, per_device(): pieces = lax.all_gather(down_local, 'tp', axis=0, tiled=False)  12.2 us
    unnamed x5, local copies, waits for them, and re-layouts  10.4 us
    dot_general x1, matrix products, per_device(): jnp.dot(hidden, down_serving, preferred_element_type=jnp.float32)  8.92 us
  transfers between devices with their start and end apart: 3, of which 2 were waited for; matrix products, arithmetic and copies ran while one was open for 12% of the time, Pallas kernels for 0%

profile of v1, /device:TPU:0, one launch (start us, length us, event | category | flops | bytes accessed | tf_op | source)
XLA Modules:
  0.0 216.8 jit_solution(9657787762168556309)
XLA Ops:
  7.2 0.0 copy-start.1
  7.2 0.0 all-gather.6.cloned.1.call-start
  7.2 3.8 %convert_element_type.19 = bf16[2048,512]{1,0:T(8,128)(2,1)} convert(f32[2048,512]{1,0:T(8,128)} %param.7) | non-fusion elementwise | flops 1048576 | bytes 6291456 | tf_op jit(solution)/shard_map/convert_element_type | solution.py:11
  11.0 0.0 all-gather.6.cloned.1.call-update
  11.0 0.0 copy-start
  11.0 0.0 all-gather.4.cloned.1.call-start
  11.1 0.0 copy-done.1
  11.1 2.5 %multiply_convert_fusion = bf16[512,2048]{1,0:T(8,128)(2,1)S(1)} fusion(f32[512,2048]{1,0:T(8,128)} %param.6, f32[512]{0:T(512)S(1)} %copy-done.1), kind=kLoop, calls=%fused_computation | loop fusion | flops 2097152 | bytes 6293504 | tf_op jit(solution)/shard_map/convert_element_type | solution.py:10
  13.6 48.1 %all_to_all.32 = bf16[4,128,2048]{2,1,0:T(8,128)(2,1)S(1)} all-to-all(bf16[4,128,2048]{2,1,0:T(8,128)(2,1)S(1)} %bitcast.25), channel_id=1, replica_groups=mesh['grp'=2,'fs'=4,'tp'=4] {'tp'}, dimensions={0} | all-to-all | bytes 4194304 | tf_op jit(solution)/shard_map/all_to_all | solution.py:14
  61.6 52.6 %all_to_all.33 = bf16[128,4,2048]{2,0,1:T(8,128)(2,1)} all-to-all(bf16[128,4,2048]{2,0,1:T(8,128)(2,1)S(1)} %bitcast.24), channel_id=1, replica_groups=mesh['grp'=2,'fs'=4,'tp'=4] {'fs'}, dimensions={1} | all-to-all | bytes 4194304 | tf_op jit(solution)/shard_map/all_to_all | solution.py:15
  114.2 0.0 all-gather.4.cloned.1.call-update
  114.2 0.0 reduce-scatter.2.cloned.1.call-start
  114.3 0.0 copy-done
  114.3 0.1 fusion.3
  114.4 0.1 fusion.4
  114.5 15.7 %all_gather.15 = bf16[128,2048]{1,0:T(8,128)(2,1)S(1)} all-gather(bf16[32,2048]{1,0:T(8,128)(2,1)S(1)} %fusion.4), channel_id=1, replica_groups=mesh['grp'=2,'fs'=4,'tp'=4] {'fs'}, dimensions={0}, use_global_device_ids=true | all-gather | bytes 655360 | tf_op jit(solution)/shard_map/all_gather | solution.py:28
  130.2 0.0 all-gather.6.cloned.1.call-done
  130.2 12.2 %copy.10 = bf16[4,2048,512]{2,0,1:T(4,128)(2,1)} copy(bf16[4,2048,512]{2,1,0:T(8,128)(2,1)} %bitcast.21) | data formatting | bytes 16777216 | tf_op jit(solution)/shard_map/all_gather | solution.py:12
  142.4 10.4 %copy.11 = bf16[256,8,4,512]{3,1,2,0:T(8,128)(2,1)} copy(bf16[256,8,4,512]{3,2,1,0:T(4,128)(2,1)} %bitcast.20) | data formatting | bytes 16777216
  152.8 18.1 %all-gather.4.cloned.1.call-done = bf16[2048,2048]{1,0:T(8,128)(2,1)} async-done(((bf16[512,2048]{1,0:T(8,128)(2,1)}), bf16[2048,2048]{1,0:T(8,128)(2,1)}) %all-gather.4.cloned.1.call-update) | async-done | bytes 8388624 | tf_op jit(solution)/shard_map/all_gather | solution.py:16
  170.9 8.4 %copy.9 = bf16[4,4,128,2048]{3,2,1,0:T(8,128)(2,1)} copy(bf16[4,4,128,2048]{3,2,0,1:T(8,128)(2,1)} %bitcast.22) | data formatting | bytes 16777216 | tf_op jit(solution)/shard_map/transpose | solution.py:22
  179.3 8.9 %convolution_convert_fusion = bf16[128,2048]{1,0:T(8,128)(2,1)} fusion(bf16[2048,2048]{1,0:T(8,128)(2,1)} %bitcast.16, bf16[128,2048]{1,0:T(8,128)(2,1)S(1)} %all_gather.15, bf16[2048,2048]{1,0:T(8,128)(2,1)} %bitcast.18), kind=kOutput, calls=%fused_computation.3 | convolution fusion | flops 2148532224 | bytes 17825792 | tf_op jit(solution)/shard_map/dot_general | solution.py:34
  188.2 0.0 reduce-scatter.2.cloned.1.call-update
  188.3 22.0 %reduce-scatter.2.cloned.1.call-done = bf16[32,2048]{1,0:T(8,128)(2,1)} async-done(((bf16[128,2048]{1,0:T(8,128)(2,1)}), bf16[32,2048]{1,0:T(8,128)(2,1)}) %reduce-scatter.2.cloned.1.call-update) | async-done | bytes 131088 | tf_op jit(solution)/shard_map/reduce_scatter | solution.py:33
  (1 shorter events, 0.0 us)
Async XLA Ops:
  7.2 3.9 %copy-start.1 = (f32[512]{0:T(512)S(1)}, f32[512]{0:T(512)}, u32[]{:S(2)}) copy-start(f32[512]{0:T(512)} %param.5) | copy-start | bytes 6148
  7.2 123.0 %all-gather.6.cloned.1.call-start = ((), (), s32[]{:S(2)}) async-start(), calls=%async_computation.5 | async-start | bytes 10485760 | tf_op jit(solution)/shard_map/all_gather | solution.py:12
  11.0 103.3 %copy-start = (bf16[32,2048]{1,0:T(8,128)(2,1)S(1)}, bf16[32,2048]{1,0:T(8,128)(2,1)}, u32[]{:S(2)}) copy-start(bf16[32,2048]{1,0:T(8,128)(2,1)} %param.4) | copy-start | bytes 393220
  11.0 159.8 %all-gather.4.cloned.1.call-start = ((), (), s32[]{:S(2)}) async-start(), calls=%async_computation.3 | async-start | bytes 10485760 | tf_op jit(solution)/shard_map/all_gather | solution.py:16
  114.2 96.0 %reduce-scatter.2.cloned.1.call-start = ((), (), s32[]{:S(2)}) async-start(), calls=%async_computation.4 | async-start | bytes 655360 | tf_op jit(solution)/shard_map/reduce_scatter | solution.py:33
Sparse Core Ops, SparseCore 0:
  11.1 78.8 all-gather.5
  114.4 56.4 all-gather.3
  188.4 21.8 reduce-scatter.1

commit v2 on v0

--- a/solution.py
+++ b/solution.py
@@ -12,7 +12,10 @@
     down_serving = lax.all_gather(down_local, "tp", axis=1, tiled=True)
     thin_rows = lax.all_to_all(folded, "tp", split_axis=0, concat_axis=1, tiled=True)
     crossed = lax.all_to_all(thin_rows, "fs", split_axis=1, concat_axis=0, tiled=True)
-    stacked = lax.all_gather(crossed, "tp", axis=0, tiled=True)
+    size = lax.axis_size("tp")
+    parts = jnp.stack([crossed for _ in range(size)])
+    parts = lax.all_to_all(parts, "tp", split_axis=0, concat_axis=0)
+    stacked = jnp.concatenate(parts, axis=0)
     tp_count = lax.axis_size("tp")
     fs_count = lax.axis_size("fs")
     slice_height = folded.shape[0] // tp_count

time: 256 us -> 271 us (1.059)
  blocking collectives: 98.1 us -> 117 us
  waiting for transfers between devices: 111 us -> 96.8 us
  starting transfers between devices: 0.12 us -> 5.86 us
  local copies, waits for them, and re-layouts: 16.9 us -> 21.3 us
    all_to_all x0 -> x1, waiting for transfers between devices: none -> 76.6 us  [per_device(): parts = lax.all_to_all(parts, 'tp', split_axis=0, concat_axis=0)]
    all_gather x1, waiting for transfers between devices: 52 us -> 0.01 us  [per_device(): down_serving = lax.all_gather(down_local, 'tp', axis=1, tiled=True)]
    all_gather x1 -> x0, waiting for transfers between devices: 37.2 us -> none  [per_device(): stacked = lax.all_gather(crossed, 'tp', axis=0, tiled=True)]
    all_to_all x1, blocking collectives: 29.7 us -> 48 us  [per_device(): lax.all_to_all(folded, 'tp', split_axis=0, concat_axis=1, tiled=True)]
    all_to_all x0 -> x1, starting transfers between devices: none -> 5.79 us  [per_device(): parts = lax.all_to_all(parts, 'tp', split_axis=0, concat_axis=0)]
    another operation x0 -> x1, local copies, waits for them, and re-layouts: none -> 4.46 us  [per_device(): parts = jnp.stack([crossed for _ in range(size)])]
    unnamed x3 -> x5, local copies, waits for them, and re-layouts: 8.44 us -> 8.45 us
  transfers between devices with their start and end apart: 3 -> 3, of which waited for: 3 -> 2; matrix products, arithmetic and copies ran while one was open for 5% -> 6% of each run, Pallas kernels for 0% -> 0%
where the time goes in v2:
time: 271 us; the launch traced here: 270 us
  blocking collectives  117 us (43%)
  waiting for transfers between devices  96.8 us (36%)
  local copies, waits for them, and re-layouts  21.3 us (8%)
  between operations  14.1 us (5%)
  matrix products  8.93 us (3%)
  other arithmetic  6.49 us (2%)
  starting transfers between devices  5.86 us (2%)
    all_to_all x1, waiting for transfers between devices, per_device(): parts = lax.all_to_all(parts, 'tp', split_axis=0, concat_axis=0)  76.6 us
    all_to_all x1, blocking collectives, per_device(): lax.all_to_all(thin_rows, 'fs', split_axis=1, concat_axis=0, tiled=True)  52.5 us
    all_to_all x1, blocking collectives, per_device(): lax.all_to_all(folded, 'tp', split_axis=0, concat_axis=1, tiled=True)  48 us
    reduce_scatter x1, waiting for transfers between devices, per_device(): lax.psum_scatter(jnp.dot(hidden, down_serving, preferred_element_type=jnp...  20.2 us
    all_gather x1, blocking collectives, per_device(): lax.all_gather(normed, 'fs', axis=0, tiled=True)  16.2 us
    dot_general x1, matrix products, per_device(): jnp.dot(hidden, down_serving, preferred_element_type=jnp.float32)  8.93 us
    unnamed x5, local copies, waits for them, and re-layouts  8.45 us
    transpose x1, local copies, waits for them, and re-layouts, per_device(): up_serving = up_serving.transpose(1, 0, 2, 3).reshape(-1, unit_count)  8.44 us
  transfers between devices with their start and end apart: 3, of which 2 were waited for; matrix products, arithmetic and copies ran while one was open for 6% of the time, Pallas kernels for 0%

profile of v2, /device:TPU:0, one launch (start us, length us, event | category | flops | bytes accessed | tf_op | source)
XLA Modules:
  0.0 270.3 jit_solution(8743239027570895288)
XLA Ops:
  7.2 0.0 copy-start.1
  7.2 0.0 all-gather.2.cloned.1.call-start
  7.2 3.8 %convert_element_type.19 = bf16[2048,512]{1,0:T(8,128)(2,1)} convert(f32[2048,512]{1,0:T(8,128)} %param.7) | non-fusion elementwise | flops 1048576 | bytes 6291456 | tf_op jit(solution)/shard_map/convert_element_type | solution.py:11
  11.0 0.0 all-gather.2.cloned.1.call-update
  11.0 0.0 copy-done.1
  11.0 2.5 multiply_convert_fusion
  13.5 48.0 %all_to_all.34 = bf16[4,128,2048]{2,1,0:T(8,128)(2,1)S(1)} all-to-all(bf16[4,128,2048]{2,1,0:T(8,128)(2,1)S(1)} %bitcast.16), channel_id=1, replica_groups=mesh['grp'=2,'fs'=4,'tp'=4] {'tp'}, dimensions={0} | all-to-all | bytes 4194304 | tf_op jit(solution)/shard_map/all_to_all | solution.py:13
  61.5 52.5 %all_to_all.35 = bf16[128,4,2048]{2,0,1:T(8,128)(2,1)S(1)} all-to-all(bf16[128,4,2048]{2,0,1:T(8,128)(2,1)S(1)} %bitcast.15), channel_id=1, replica_groups=mesh['grp'=2,'fs'=4,'tp'=4] {'fs'}, dimensions={1} | all-to-all | bytes 4194304 | tf_op jit(solution)/shard_map/all_to_all | solution.py:14
  114.0 4.5 %stack.10 = bf16[4,512,2048]{2,1,0:T(8,128)(2,1)} broadcast(bf16[512,2048]{1,0:T(8,128)(2,1)S(1)} %bitcast.14), dimensions={1,2} | broadcast | bytes 10485760 | tf_op jit(solution)/shard_map/stack | solution.py:16
  118.4 0.0 copy-start
  118.4 5.8 %all-to-all-start.2 = ((bf16[4,512,2048]{2,1,0:T(8,128)(2,1)}), bf16[4,512,2048]{2,1,0:T(8,128)(2,1)}, u32[]{:S(2)}, u32[]{:S(2)}) async-start(bf16[4,512,2048]{2,1,0:T(8,128)(2,1)} %stack.10), calls=%async_computation.2 | async-start | bytes 16777216 | tf_op jit(solution)/shard_map/all_to_all | solution.py:17
  124.2 0.0 reduce-scatter.2.cloned.1.call-start
  124.3 0.0 copy-done
  124.3 0.1 fusion.3
  124.5 0.1 fusion.4
  124.6 16.2 %all_gather.7 = bf16[128,2048]{1,0:T(8,128)(2,1)S(1)} all-gather(bf16[32,2048]{1,0:T(8,128)(2,1)S(1)} %fusion.4), channel_id=1, replica_groups=mesh['grp'=2,'fs'=4,'tp'=4] {'fs'}, dimensions={0}, use_global_device_ids=true | all-gather | bytes 655360 | tf_op jit(solution)/shard_map/all_gather | solution.py:30
  140.8 76.6 %all-to-all-done.2 = bf16[4,512,2048]{2,1,0:T(8,128)(2,1)} async-done(((bf16[4,512,2048]{2,1,0:T(8,128)(2,1)}), bf16[4,512,2048]{2,1,0:T(8,128)(2,1)}, u32[]{:S(2)}, u32[]{:S(2)}) %all-to-all-start.2) | async-done | bytes 8388640 | tf_op jit(solution)/shard_map/all_to_all | solution.py:17
  217.4 8.4 %copy.7 = bf16[4,4,128,2048]{3,2,1,0:T(8,128)(2,1)} copy(bf16[4,4,128,2048]{3,2,0,1:T(8,128)(2,1)} %bitcast.5) | data formatting | bytes 16777216 | tf_op jit(solution)/shard_map/transpose | solution.py:24
  225.8 0.0 all-gather.2.cloned.1.call-done
  225.8 8.9 %convolution_convert_fusion = bf16[128,2048]{1,0:T(8,128)(2,1)} fusion(bf16[2048,2048]{1,0:T(8,128)(2,1)} %all-gather.2.cloned.1.call-done, bf16[128,2048]{1,0:T(8,128)(2,1)S(1)} %all_gather.7, bf16[2048,2048]{1,0:T(8,128)(2,1)} %bitcast.12), kind=kOutput, calls=%fused_computation.3 | convolution fusion | flops 2148532224 | bytes 17825792 | tf_op jit(solution)/shard_map/dot_general | solution.py:36
  234.8 0.0 reduce-scatter.2.cloned.1.call-update
  234.8 20.2 %reduce-scatter.2.cloned.1.call-done = bf16[32,2048]{1,0:T(8,128)(2,1)} async-done(((bf16[128,2048]{1,0:T(8,128)(2,1)}), bf16[32,2048]{1,0:T(8,128)(2,1)}) %reduce-scatter.2.cloned.1.call-update) | async-done | bytes 131088 | tf_op jit(solution)/shard_map/reduce_scatter | solution.py:35
  255.0 8.4 %copy.9 = bf16[2048,2048]{1,0:T(8,128)(2,1)} copy(bf16[2048,2048]{1,0:T(8,128)(2,1)} %all-gather.2.cloned.1.call-done) | data formatting | bytes 16777216
  (1 shorter events, 0.0 us)
Async XLA Ops:
  7.2 3.9 %copy-start.1 = (f32[512]{0:T(512)S(1)}, f32[512]{0:T(512)}, u32[]{:S(2)}) copy-start(f32[512]{0:T(512)} %param.5) | copy-start | bytes 6148
  7.2 218.7 %all-gather.2.cloned.1.call-start = ((), (), s32[]{:S(2)}) async-start(), calls=%async_computation.4 | async-start | bytes 10485760 | tf_op jit(solution)/shard_map/all_gather | solution.py:12
  118.4 5.8 %copy-start = (bf16[32,2048]{1,0:T(8,128)(2,1)S(1)}, bf16[32,2048]{1,0:T(8,128)(2,1)}, u32[]{:S(2)}) copy-start(bf16[32,2048]{1,0:T(8,128)(2,1)} %param.4) | copy-start | bytes 393220
  118.4 98.9 %all-to-all-start.2 = ((bf16[4,512,2048]{2,1,0:T(8,128)(2,1)}), bf16[4,512,2048]{2,1,0:T(8,128)(2,1)}, u32[]{:S(2)}, u32[]{:S(2)}) async-start(bf16[4,512,2048]{2,1,0:T(8,128)(2,1)} %stack.10), calls=%async_computation.2 | async-start | bytes 16777216 | tf_op jit(solution)/shard_map/all_to_all | solution.py:17
  124.2 130.8 %reduce-scatter.2.cloned.1.call-start = ((), (), s32[]{:S(2)}) async-start(), calls=%async_computation.5 | async-start | bytes 655360 | tf_op jit(solution)/shard_map/reduce_scatter | solution.py:35
Sparse Core Ops, SparseCore 0:
  11.1 78.7 all-gather.1
  234.9 20.0 reduce-scatter.1
